TPU v7x, 512 devices: a whole 4x8x8 slice. The times are simulated.
512 devices in a mesh: ep: 32 (over z, x), tp: 16 (over y, core).
Axes of the slice: x: 4, y: 8, z: 8, core: 2. Of those that a mesh axis runs over, the one named last changes fastest.
Arguments:
- mixer_rows: bfloat16 [4096, 2048], P('ep'), may hold values from -40 to 40
- mixer_gain: float32 [2048], replicated, may hold values from 0.1 to 1.9
- inner_weight: bfloat16 [2048, 1024], P(None, 'tp'), may hold values from -0.125 to 0.125
- gate_in_weight: bfloat16 [2048, 1024], P(None, 'tp'), may hold values from -0.125 to 0.125
- gate_out_weight: bfloat16 [2048, 1024], P(None, 'tp'), may hold values from -0.125 to 0.125
- conv_taps: float32 [3, 1024], P(None, 'tp'), may hold values from -3.5 to 3.5
- mixer_out_weight: bfloat16 [1024, 2048], P('tp'), may hold values from -0.1875 to 0.1875
- routed_rows: bfloat16 [8192, 2048], P('ep'), may hold values from -40 to 40
- routed_gain: float32 [2048], replicated, may hold values from 0.1 to 1.9
- route_ids: int32 [8192, 2], P('ep'), may hold values from 0 to 31, all different within a row; in each aligned block of 256 rows (0 to 255, 256 to 511, ...) at most 32 rows name the same one
- route_weights: float32 [8192, 2], P('ep'), may hold values from 0.25 to 1
- expert_gate: bfloat16 [32, 2048, 2048], P('ep', None, 'tp'), may hold values from -0.125 to 0.125
- expert_up: bfloat16 [32, 2048, 2048], P('ep', None, 'tp'), may hold values from -0.125 to 0.125
- expert_down: bfloat16 [32, 2048, 2048], P('ep', 'tp'), may hold values from -0.125 to 0.125
Outputs:
- mixer_output: bfloat16 [4096, 2048], P('ep')
- routed_output: bfloat16 [8192, 2048], P('ep')
Inputs may be any that keep to these rules, and one draw needn't show every extreme that they name: `route_ids`: within each aligned block of 256 tokens, no expert is named by more than 32 choices, a bound that some block reaches; a token's 2 experts differ.
All inputs are finite; a program needn't handle non-finite values.
Results may differ from a plain program's by a relative error of at most 0.019.
Values may be sent and summed in bfloat16 or wider, within the bound.
A program may use at most 64 MiB of HBM per device.

v0:
```python
import jax
import jax.numpy as jnp
from jax import lax
from jax.sharding import PartitionSpec as P


def shifted(value, axis, steps):
    count = lax.axis_size(axis)
    initial, last = (max(0, -steps), min(count, count - steps))
    return lax.ppermute(value, axis, [(source, source + steps) for source in range(initial, last)])


def packed_total(arrays, axis):
    ends = [0]
    for a in arrays:
        ends.append(ends[-1] + a.size)
    so_far = lax.psum(jnp.concatenate([a.ravel() for a in arrays]), axis)
    return tuple((so_far[b:e].reshape(a.shape) for a, b, e in zip(arrays, ends, ends[1:])))


def rms_scale(row_block, gain_row):
    values = row_block.astype(jnp.float32)
    scaled = values * lax.rsqrt(jnp.mean(values * values, axis=-1, keepdims=True) + 1e-06)
    return (scaled * gain_row).astype(jnp.bfloat16)


def on_device(
    mixer_rows,
    mixer_gain,
    inner_weight,
    gate_in_weight,
    gate_out_weight,
    conv_taps,
    mixer_out_weight,
    routed_rows,
    routed_gain,
    route_ids,
    route_weights,
    expert_gate,
    expert_up,
    expert_down,
):
    normed = rms_scale(mixer_rows, mixer_gain)
    inner_proj = jnp.dot(normed, inner_weight, preferred_element_type=jnp.float32)
    gate_in = jnp.dot(normed, gate_in_weight, preferred_element_type=jnp.float32)
    conv_input = (gate_in * inner_proj).astype(jnp.bfloat16)
    gate_out = jnp.dot(normed, gate_out_weight, preferred_element_type=jnp.float32)
    tap_total = conv_taps.shape[0]
    rim_rows = tap_total - 1
    earlier_rows = shifted(conv_input[conv_input.shape[0] - rim_rows :], "ep", 1)
    extended = jnp.concatenate([earlier_rows, conv_input], axis=0).astype(jnp.float32)
    length = conv_input.shape[0]
    conv_out = jnp.zeros(conv_input.shape, jnp.float32)
    for tap_index in range(tap_total):
        conv_out = conv_out + conv_taps[tap_index] * extended[tap_index : tap_index + length]
    gated_conv = (gate_out * conv_out).astype(jnp.bfloat16)
    mixer_terms = jnp.dot(gated_conv, mixer_out_weight, preferred_element_type=jnp.float32)
    routed_normed = rms_scale(routed_rows, routed_gain)
    experts = lax.axis_size("ep")
    groups = lax.axis_size("tp")
    column = lax.axis_index("tp")
    tok_count, pick_count = route_ids.shape
    model_width = routed_rows.shape[1]
    capacity = 2 * tok_count * pick_count // experts
    share_rows = capacity // groups
    flat_ids = route_ids.reshape(-1)
    onehot = (flat_ids[:, None] == jnp.arange(experts, dtype=jnp.int32)[None, :]).astype(jnp.int32)
    slot_rank = jnp.sum((jnp.cumsum(onehot, axis=0) - onehot) * onehot, axis=1)
    slot_number = slot_rank * experts + flat_ids
    owners = jnp.arange(tok_count * pick_count, dtype=jnp.int32) // pick_count
    matches = slot_number[None, :] == jnp.arange(capacity * experts, dtype=jnp.int32)[:, None]
    token_table = jnp.where(
        jnp.any(matches, axis=1), jnp.sum(jnp.where(matches, owners[None, :], 0), axis=1), tok_count
    )
    padded_rows = jnp.concatenate(
        [routed_normed, jnp.zeros((1, model_width), jnp.bfloat16)], axis=0
    )
    table_share = lax.dynamic_slice_in_dim(
        token_table.reshape(capacity, experts), column * share_rows, share_rows, 0
    )
    outgoing = jnp.take(padded_rows, table_share.reshape(-1), axis=0).reshape(
        share_rows, experts, model_width
    )
    arrived = lax.all_to_all(outgoing, "ep", split_axis=1, concat_axis=1, tiled=True)
    incoming = lax.all_gather(arrived, "tp", axis=0, tiled=True)
    slot_rows = incoming.reshape(capacity * experts, model_width)
    gate_act = jnp.dot(slot_rows, expert_gate[0], preferred_element_type=jnp.float32)
    up_act = jnp.dot(slot_rows, expert_up[0], preferred_element_type=jnp.float32)
    hidden = (jax.nn.silu(gate_act) * up_act).astype(jnp.bfloat16)
    summed = lax.psum_scatter(
        jnp.dot(hidden, expert_down[0], preferred_element_type=jnp.float32).astype(jnp.bfloat16),
        "tp",
        scatter_dimension=0,
        tiled=True,
    )
    returned = lax.all_to_all(
        summed.reshape(share_rows, experts, model_width),
        "ep",
        split_axis=1,
        concat_axis=1,
        tiled=True,
    )
    flat_back = jnp.concatenate(
        [
            returned.reshape(share_rows * experts, model_width),
            jnp.zeros((1, model_width), jnp.bfloat16),
        ],
        axis=0,
    )
    local_slot = jnp.where(
        slot_rank // share_rows == column,
        (slot_rank - column * share_rows) * experts + flat_ids,
        share_rows * experts,
    )
    contrib = (
        jnp.take(flat_back, local_slot, axis=0).astype(jnp.float32)
        * route_weights.reshape(-1)[:, None]
    )
    routed_terms = jnp.sum(contrib.reshape(tok_count, pick_count, model_width), axis=1)
    mixer_total, routed_total = tuple(
        (
            part.astype(jnp.float32)
            for part in packed_total(
                (mixer_terms.astype(jnp.bfloat16), routed_terms.astype(jnp.bfloat16)), "tp"
            )
        )
    )
    return (mixer_total.astype(jnp.bfloat16), routed_total.astype(jnp.bfloat16))


def solution(mesh):
    return jax.shard_map(
        on_device,
        mesh=mesh,
        in_specs=(
            P("ep", None),
            P(),
            P(None, "tp"),
            P(None, "tp"),
            P(None, "tp"),
            P(None, "tp"),
            P("tp", None),
            P("ep", None),
            P(),
            P("ep", None),
            P("ep", None),
            P("ep", None, "tp"),
            P("ep", None, "tp"),
            P("ep", "tp", None),
        ),
        out_specs=(P("ep", None), P("ep", None)),
        check_vma=False,
    )
```

profile of v0, /device:TPU:1, one launch (start us, length us, event | category | flops | bytes accessed | tf_op | source)
XLA Modules:
  0.0 321.4 jit_solution(4402862292982536007)
XLA Ops:
  7.2 0.9 copy.70
  8.2 0.1 eq.62
  8.3 0.1 eq.58
  8.5 1.2 reduce-window.6
  9.6 0.2 slice_reduce_fusion
  9.9 0.1 fusion.24
  10.0 0.3 fusion.3
  10.3 0.3 select_reduce_fusion
  10.7 0.1 reshape.246
  10.8 1.5 fusion
  12.3 0.1 copy.79
  12.4 1.0 fusion.2
  13.4 0.1 concatenate.13
  13.5 0.7 gather_fusion
  14.3 0.3 broadcast_select_fusion.1
  14.6 24.8 %all_to_all.10 = bf16[2,32,2048]{2,0,1:T(2,128)(2,1)S(1)} all-to-all(bf16[2,32,2048]{2,0,1:T(2,128)(2,1)S(1)} %broadcast_select_fusion.1), channel_id=1, replica_groups=mesh['ep'=32,'tp'=16] {'ep'}, dimensions={1} | all-to-all | bytes 524288 | tf_op jit(solution)/shard_map/all_to_all | solution.py:84
  39.5 0.8 copy.81
  40.3 42.1 %all-gather.2.cloned.1.call-done = bf16[32,32,2048]{2,1,0:T(8,128)(2,1)} async-done(((bf16[2,32,2048]{2,1,0:T(8,128)(2,1)}), bf16[32,32,2048]{2,1,0:T(8,128)(2,1)}) %all-gather.2.cloned.1.call-update) | async-done | bytes 4194320 | tf_op jit(solution)/shard_map/all_gather | solution.py:85
  82.4 3.5 %fusion.14 = f32[1024,128]{1,0:T(8,128)S(1)} fusion(bf16[1024,2048]{1,0:T(8,128)(2,1)} %bitcast.56, bf16[1,2048,128]{2,1,0:T(8,128)(2,1)S(1)} %copy-done.3), kind=kOutput, calls=%fused_computation.30 | convolution fusion | flops 536870912 | bytes 5242880 | tf_op jit(solution)/shard_map/dot_general | solution.py:87
  86.0 8.5 %convolution_convert_fusion = bf16[1024,2048]{1,0:T(8,128)(2,1)} fusion(bf16[1024,2048]{1,0:T(8,128)(2,1)} %bitcast.57, bf16[1,128,2048]{2,1,0:T(8,128)(2,1)S(1)} %copy-done, bf16[1,2048,128]{2,1,0:T(8,128)(2,1)S(1)} %copy-done.4, f32[1024,128]{1,0:T(8,128)S(1)} %fusion.14), kind=kOutput, calls=%fused_computation.4 | convolution fusion | flops 1076625408 | bytes 9961472 | tf_op jit(solution)/shard_map/dot_general | solution.py:91
  94.5 1.0 copy-done.2
  95.5 0.2 fusion.8
  95.7 0.4 fusion.39
  96.1 0.4 fusion.7
  96.5 0.1 slice.70
  96.5 3.1 collective-permute-start
  99.6 0.1 reshape.250
  99.8 0.1 reduce_sum.51
  100.1 56.6 %reduce-scatter.2.cloned.1.call-done = bf16[64,2048]{1,0:T(8,128)(2,1)} async-done(((bf16[1024,2048]{1,0:T(8,128)(2,1)}), bf16[64,2048]{1,0:T(8,128)(2,1)}) %reduce-scatter.2.cloned.1.call-update) | async-done | bytes 262160 | tf_op jit(solution)/shard_map/reduce_scatter | solution.py:90
  156.7 1.9 copy.82
  158.6 9.1 %all-to-all-start.1 = ((bf16[2,32,2048]{2,0,1:T(2,128)(2,1)}), bf16[2,32,2048]{2,0,1:T(2,128)(2,1)S(1)}, u32[]{:S(2)}, u32[]{:S(2)}) async-start(bf16[2,32,2048]{2,0,1:T(2,128)(2,1)} %copy.82), calls=%async_computation.2 | async-start | bytes 524288 | tf_op jit(solution)/shard_map/all_to_all | solution.py:96
  167.7 0.2 all-reduce.4.cloned.1.call-start
  167.9 0.2 copy.78
  168.1 0.8 copy.85
  168.9 0.1 maximum_convert_fusion
  169.0 0.9 fusion.4
  170.0 0.1 copy.87
  170.1 8.1 %all-to-all-done.1 = bf16[2,32,2048]{2,0,1:T(2,128)(2,1)S(1)} async-done(((bf16[2,32,2048]{2,0,1:T(2,128)(2,1)}), bf16[2,32,2048]{2,0,1:T(2,128)(2,1)S(1)}, u32[]{:S(2)}, u32[]{:S(2)}) %all-to-all-start.1) | async-done | bytes 262176 | tf_op jit(solution)/shard_map/all_to_all | solution.py:96
  178.2 0.1 copy.83
  178.3 2.5 gather_fusion.1
  180.8 2.7 gather.15
  183.4 9.9 %multiply_reduce_fusion = bf16[256,2048]{1,0:T(8,128)(2,1)S(1)} fusion(bf16[256,2,2048]{2,1,0:T(2,128)(2,1)} %gather.15, pred[256,2]{1,0:T(8,128)(4,1)S(1)} %copy.78, f32[256,2]{1,0:T(8,128)S(1)} %copy-done.5), kind=kLoop, calls=%fused_computation.2 | loop fusion | flops 3670016 | bytes 3148288 | tf_op jit(solution)/shard_map/reduce_sum | solution.py:119
  193.3 0.2 copy.88
  193.5 1.3 pad_maximum_fusion
  194.8 116.5 %all-reduce.4.cloned.1.call-done = bf16[786432]{0:T(1024)(128)(2,1)} async-done(((bf16[786432]{0:T(1024)(128)(2,1)}), bf16[786432]{0:T(1024)(128)(2,1)}) %all-reduce.4.cloned.1.call-update) | async-done | bytes 1572880 | tf_op jit(solution)/shard_map/psum | solution.py:17
  311.4 1.2 slice-done
  312.6 1.3 slice.65
  313.8 1.0 slice.63
  (53 shorter events, 0.5 us)
Async XLA Ops:
  7.2 78.8 %copy-start = (bf16[1,128,2048]{2,1,0:T(8,128)(2,1)S(1)}, bf16[1,128,2048]{2,1,0:T(8,128)(2,1)}, u32[]{:S(2)}) copy-start(bf16[1,128,2048]{2,1,0:T(8,128)(2,1)} %param.27) | copy-start | bytes 1572868
  7.2 5.3 %copy-start.1 = (bf16[256,2048]{1,0:T(8,128)(2,1)S(1)}, bf16[256,2048]{1,0:T(8,128)(2,1)}, u32[]{:S(2)}) copy-start(bf16[256,2048]{1,0:T(8,128)(2,1)} %param.21) | copy-start | bytes 3145732
  7.2 75.2 %all-gather.2.cloned.1.call-start = ((), (), s32[]{:S(2)}) async-start(), calls=%async_computation.3 | async-start | bytes 4456448 | tf_op jit(solution)/shard_map/all_gather | solution.py:85
  13.5 68.9 %copy-start.3 = (bf16[1,2048,128]{2,1,0:T(8,128)(2,1)S(1)}, bf16[1,2048,128]{2,1,0:T(8,128)(2,1)}, u32[]{:S(2)}) copy-start(bf16[1,2048,128]{2,1,0:T(8,128)(2,1)} %param.25) | copy-start | bytes 1572868
  40.3 116.4 %reduce-scatter.2.cloned.1.call-start = ((), (), s32[]{:S(2)}) async-start(), calls=%async_computation.4 | async-start | bytes 4456448 | tf_op jit(solution)/shard_map/reduce_scatter | solution.py:90
  82.4 3.5 %copy-start.4 = (bf16[1,2048,128]{2,1,0:T(8,128)(2,1)S(1)}, bf16[1,2048,128]{2,1,0:T(8,128)(2,1)}, u32[]{:S(2)}) copy-start(bf16[1,2048,128]{2,1,0:T(8,128)(2,1)} %param.26) | copy-start | bytes 1572868
  94.4 1.0 copy-start.2
  94.4 1.3 copy-start.8
  94.4 1.3 copy-start.12
  94.4 1.7 copy-start.13
  95.5 4.5 %copy-start.9 = (s32[256,2]{0,1:T(2,128)S(1)}, s32[256,2]{0,1:T(2,128)}, u32[]{:S(2)}) copy-start(s32[256,2]{0,1:T(2,128)} %param.23) | copy-start | bytes 6148
  95.5 72.4 %copy-start.11 = (f32[3,64]{1,0:T(4,128)S(1)}, f32[3,64]{1,0:T(4,128)}, u32[]{:S(2)}) copy-start(f32[3,64]{1,0:T(4,128)} %param.19) | copy-start | bytes 2308
  95.5 72.7 %copy-start.10 = (f32[256,2]{0,1:T(2,128)S(1)}, f32[256,2]{0,1:T(2,128)}, u32[]{:S(2)}) copy-start(f32[256,2]{0,1:T(2,128)} %param.24) | copy-start | bytes 6148
  95.7 73.4 %copy-start.6 = (bf16[64,2048]{1,0:T(8,128)(2,1)S(1)}, bf16[64,2048]{1,0:T(8,128)(2,1)}, u32[]{:S(2)}) copy-start(bf16[64,2048]{1,0:T(8,128)(2,1)} %param.20) | copy-start | bytes 786436
  95.7 73.4 %copy-start.7 = (bf16[2048,64]{0,1:T(8,128)(2,1)S(1)}, bf16[2048,64]{0,1:T(8,128)(2,1)}, u32[]{:S(2)}) copy-start(bf16[2048,64]{0,1:T(8,128)(2,1)} %param.18) | copy-start | bytes 786436
  96.5 72.4 %collective-permute-start = (bf16[2,64]{0,1:T(8,128)(2,1)S(1)}, bf16[2,64]{0,1:T(8,128)(2,1)S(1)}, u32[]{:S(2)}, u32[]{:S(2)}) collective-permute-start(bf16[2,64]{0,1:T(8,128)(2,1)S(1)} %slice.70), channel_id=1, source_target_pairs={{0,16},{16,32},{32,48},{48,64},{64,80},{80,96},{96,112},{112,128},... | collective-permute-start | bytes 776 | tf_op jit(solution)/shard_map/ppermute | solution.py:10
  158.6 19.6 %all-to-all-start.1 = ((bf16[2,32,2048]{2,0,1:T(2,128)(2,1)}), bf16[2,32,2048]{2,0,1:T(2,128)(2,1)S(1)}, u32[]{:S(2)}, u32[]{:S(2)}) async-start(bf16[2,32,2048]{2,0,1:T(2,128)(2,1)} %copy.82), calls=%async_computation.2 | async-start | bytes 524288 | tf_op jit(solution)/shard_map/all_to_all | solution.py:96
  167.7 143.7 %all-reduce.4.cloned.1.call-start = ((), (), s32[]{:S(2)}) async-start(), calls=%async_computation.5 | async-start | bytes 3145728 | tf_op jit(solution)/shard_map/psum | solution.py:17
  180.8 2.7 copy-start.5
  311.3 1.2 slice-start
  312.6 1.3 slice-start.1
Sparse Core Ops, SparseCore 0:
  40.4 42.0 all-gather.1
  94.6 62.0 reduce-scatter.1
  194.9 116.3 all-reduce.3
where the time goes:
time: 322 us; the launch traced here: 321 us
  waiting for transfers between devices  223 us (69%)
  blocking collectives  24.8 us (8%)
  local copies, waits for them, and re-layouts  16.8 us (5%)
  other arithmetic  16.3 us (5%)
  between operations  14.1 us (4%)
  matrix products  13.6 us (4%)
  starting transfers between devices  12.5 us (4%)
    psum x1, waiting for transfers between devices, packed_total(): so_far = lax.psum(jnp.concatenate([a.ravel() for a in arrays]), axis)  117 us
    reduce_scatter x1, waiting for transfers between devices, on_device(): lax.psum_scatter(jnp.dot(hidden, expert_down[0], preferred_element_type=j...  56.6 us
    all_gather x1, waiting for transfers between devices, on_device(): incoming = lax.all_gather(arrived, 'tp', axis=0, tiled=True)  42.1 us
    all_to_all x1, blocking collectives, on_device(): lax.all_to_all(outgoing, 'ep', split_axis=1, concat_axis=1, tiled=True)  24.8 us
    reduce_sum x1, other arithmetic, on_device(): jnp.sum(contrib.reshape(tok_count, pick_count, model_width), axis=1)  9.87 us
    all_to_all x1, starting transfers between devices, on_device(): lax.all_to_all(summed.reshape(share_rows, experts, model_width), 'ep', sp...  9.09 us
    dot_general x1, matrix products, on_device(): jnp.dot(hidden, expert_down[0], preferred_element_type=jnp.float32)  8.47 us
    all_to_all x1, waiting for transfers between devices, on_device(): lax.all_to_all(summed.reshape(share_rows, experts, model_width), 'ep', sp...  8.08 us
  transfers between devices with their start and end apart: 5, of which 4 were waited for; matrix products, arithmetic and copies ran while one was open for 2% of the time, Pallas kernels for 0%

commit v1 on v0

--- a/solution.py
+++ b/solution.py
@@ -14,7 +14,7 @@
     ends = [0]
     for a in arrays:
         ends.append(ends[-1] + a.size)
-    so_far = lax.psum(jnp.concatenate([a.ravel() for a in arrays]), axis)
+    so_far = jnp.sum(lax.all_gather(jnp.concatenate([a.ravel() for a in arrays]), axis), axis=0)
     return tuple((so_far[b:e].reshape(a.shape) for a, b, e in zip(arrays, ends, ends[1:])))
 
 

time: 322 us -> 402 us (1.25)
  other arithmetic: 16.3 us -> 49.1 us
  local copies, waits for them, and re-layouts: 16.8 us -> 44.5 us
  waiting for transfers between devices: 223 us -> 243 us
    all_gather x0 -> x1, waiting for transfers between devices: none -> 135 us  [packed_total(): lax.all_gather(jnp.concatenate([a.ravel() for a in arrays]), axis)]
    psum x1 -> x0, waiting for transfers between devices: 117 us -> none  [packed_total(): so_far = lax.psum(jnp.concatenate([a.ravel() for a in arrays]), axis)]
    reduce_sum x0 -> x1, other arithmetic: none -> 32.8 us  [packed_total(): jnp.sum(lax.all_gather(jnp.concatenate([a.ravel() for a in arrays]), axis...]
    all_gather x0 -> x1, local copies, waits for them, and re-layouts: none -> 28.7 us  [packed_total(): lax.all_gather(jnp.concatenate([a.ravel() for a in arrays]), axis)]
  transfers between devices with their start and end apart: 5 -> 5, of which waited for: 4 -> 4; matrix products, arithmetic and copies ran while one was open for 2% -> 1% of each run, Pallas kernels for 0% -> 0%
where the time goes in v1:
time: 402 us; the launch traced here: 401 us
  waiting for transfers between devices  243 us (60%)
  other arithmetic  49.1 us (12%)
  local copies, waits for them, and re-layouts  44.5 us (11%)
  blocking collectives  24.8 us (6%)
  between operations  14.1 us (4%)
  matrix products  13.6 us (3%)
  starting transfers between devices  12.1 us (3%)
    all_gather x1, waiting for transfers between devices, packed_total(): lax.all_gather(jnp.concatenate([a.ravel() for a in arrays]), axis)  135 us
    reduce_scatter x1, waiting for transfers between devices, on_device(): lax.psum_scatter(jnp.dot(hidden, expert_down[0], preferred_element_type=j...  56.8 us
    all_gather x1, waiting for transfers between devices, on_device(): incoming = lax.all_gather(arrived, 'tp', axis=0, tiled=True)  42.1 us
    reduce_sum x1, other arithmetic, packed_total(): jnp.sum(lax.all_gather(jnp.concatenate([a.ravel() for a in arrays]), axis...  32.8 us
    all_gather x1, local copies, waits for them, and re-layouts, packed_total(): lax.all_gather(jnp.concatenate([a.ravel() for a in arrays]), axis)  28.7 us
    all_to_all x1, blocking collectives, on_device(): lax.all_to_all(outgoing, 'ep', split_axis=1, concat_axis=1, tiled=True)  24.8 us
    reduce_sum x1, other arithmetic, on_device(): jnp.sum(contrib.reshape(tok_count, pick_count, model_width), axis=1)  9.87 us
    all_to_all x1, waiting for transfers between devices, on_device(): lax.all_to_all(summed.reshape(share_rows, experts, model_width), 'ep', sp...  8.73 us
  transfers between devices with their start and end apart: 5, of which 4 were waited for; matrix products, arithmetic and copies ran while one was open for 1% of the time, Pallas kernels for 0%

profile of v1, /device:TPU:1, one launch (start us, length us, event | category | flops | bytes accessed | tf_op | source)
XLA Modules:
  0.0 401.4 jit_solution(1957484743586592318)
XLA Ops:
  7.2 0.9 copy.70
  8.2 0.1 eq.58
  8.3 0.1 eq.62
  8.5 1.5 fusion
  10.0 1.2 reduce-window.6
  11.2 0.2 slice_reduce_fusion
  11.4 0.1 fusion.24
  11.6 0.3 fusion.3
  11.8 0.3 select_reduce_fusion
  12.2 0.1 reshape.246
  12.3 0.1 copy.79
  12.4 1.0 fusion.2
  13.5 0.7 gather_fusion
  14.3 0.3 broadcast_select_fusion.1
  14.6 24.8 %all_to_all.10 = bf16[2,32,2048]{2,0,1:T(2,128)(2,1)S(1)} all-to-all(bf16[2,32,2048]{2,0,1:T(2,128)(2,1)S(1)} %broadcast_select_fusion.1), channel_id=1, replica_groups=mesh['ep'=32,'tp'=16] {'ep'}, dimensions={1} | all-to-all | bytes 524288 | tf_op jit(solution)/shard_map/all_to_all | solution.py:84
  39.5 0.8 copy.81
  40.3 42.1 %all-gather.4.cloned.1.call-done = bf16[32,32,2048]{2,1,0:T(8,128)(2,1)} async-done(((bf16[2,32,2048]{2,1,0:T(8,128)(2,1)}), bf16[32,32,2048]{2,1,0:T(8,128)(2,1)}) %all-gather.4.cloned.1.call-update) | async-done | bytes 4194320 | tf_op jit(solution)/shard_map/all_gather | solution.py:85
  82.4 3.5 fusion.14
  86.0 8.5 %convolution_convert_fusion = bf16[1024,2048]{1,0:T(8,128)(2,1)} fusion(bf16[1024,2048]{1,0:T(8,128)(2,1)} %bitcast.57, bf16[1,128,2048]{2,1,0:T(8,128)(2,1)S(1)} %copy-done, bf16[1,2048,128]{2,1,0:T(8,128)(2,1)S(1)} %copy-done.6, f32[1024,128]{1,0:T(8,128)S(1)} %fusion.14), kind=kOutput, calls=%fused_computation.4 | convolution fusion | flops 1076625408 | bytes 9961472 | tf_op jit(solution)/shard_map/dot_general | solution.py:91
  94.4 1.0 copy-done.3
  95.5 0.2 fusion.8
  95.7 0.4 fusion.39
  96.1 0.4 fusion.7
  96.5 3.1 collective-permute-start
  99.6 0.1 reshape.250
  99.8 0.1 reduce_sum.63
  100.1 56.8 %reduce-scatter.2.cloned.1.call-done = bf16[64,2048]{1,0:T(8,128)(2,1)} async-done(((bf16[1024,2048]{1,0:T(8,128)(2,1)}), bf16[64,2048]{1,0:T(8,128)(2,1)}) %reduce-scatter.2.cloned.1.call-update) | async-done | bytes 262160 | tf_op jit(solution)/shard_map/reduce_scatter | solution.py:90
  156.8 1.9 copy.82
  158.8 8.7 %all-to-all-start.1 = ((bf16[2,32,2048]{2,0,1:T(2,128)(2,1)}), bf16[2,32,2048]{2,0,1:T(2,128)(2,1)S(1)}, u32[]{:S(2)}, u32[]{:S(2)}) async-start(bf16[2,32,2048]{2,0,1:T(2,128)(2,1)} %copy.82), calls=%async_computation.2 | async-start | bytes 524288 | tf_op jit(solution)/shard_map/all_to_all | solution.py:96
  167.5 0.2 all-gather.6.cloned.1.call-start
  167.8 0.2 copy.78
  168.0 0.1 copy.85
  168.1 0.1 maximum_convert_fusion
  168.2 0.9 fusion.4
  169.1 0.1 copy.87
  169.3 8.7 %all-to-all-done.1 = bf16[2,32,2048]{2,0,1:T(2,128)(2,1)S(1)} async-done(((bf16[2,32,2048]{2,0,1:T(2,128)(2,1)}), bf16[2,32,2048]{2,0,1:T(2,128)(2,1)S(1)}, u32[]{:S(2)}, u32[]{:S(2)}) %all-to-all-start.1) | async-done | bytes 262176 | tf_op jit(solution)/shard_map/all_to_all | solution.py:96
  178.0 0.1 copy.83
  178.1 2.5 gather_fusion.1
  180.6 2.7 gather.15
  183.2 9.9 %multiply_reduce_fusion = bf16[256,2048]{1,0:T(8,128)(2,1)S(1)} fusion(bf16[256,2,2048]{2,1,0:T(2,128)(2,1)} %gather.15, pred[256,2]{1,0:T(8,128)(4,1)S(1)} %copy.78, f32[256,2]{1,0:T(8,128)S(1)} %copy.85), kind=kLoop, calls=%fused_computation.2 | loop fusion | flops 3670016 | bytes 3148288 | tf_op jit(solution)/shard_map/reduce_sum | solution.py:119
  193.1 0.2 copy.88
  193.3 1.3 pad_maximum_fusion
  194.7 135.4 %all-gather.6.cloned.1.call-done = bf16[12582912]{0:T(1024)(128)(2,1)} async-done(((bf16[786432]{0:T(1024)(128)(2,1)}), bf16[12582912]{0:T(1024)(128)(2,1)}) %all-gather.6.cloned.1.call-update) | async-done | bytes 25165840 | tf_op jit(solution)/shard_map/all_gather | solution.py:17
  330.1 28.7 %reshape.267 = bf16[16,786432]{1,0:T(8,128)(2,1)} reshape(bf16[12582912]{0:T(1024)(128)(2,1)} %all-gather.6.cloned.1.call-done) | data formatting | bytes 50331648 | tf_op jit(solution)/shard_map/all_gather | solution.py:17
  358.8 32.8 %reduce_sum.68 = bf16[786432]{0:T(1024)(128)(2,1)S(1)} reduce(bf16[16,786432]{1,0:T(8,128)(2,1)} %reshape.267, bf16[]{:T(256)} %constant.82.clone.1), dimensions={0}, to_apply=%region_9.10 | reduce | flops 11796480 | bytes 26738690 | tf_op jit(solution)/shard_map/reduce_sum | solution.py:17
  391.6 0.8 slice.75
  392.6 1.3 slice.65
  393.8 1.0 slice.63
  (55 shorter events, 0.8 us)
Async XLA Ops:
  7.2 78.8 %copy-start = (bf16[1,128,2048]{2,1,0:T(8,128)(2,1)S(1)}, bf16[1,128,2048]{2,1,0:T(8,128)(2,1)}, u32[]{:S(2)}) copy-start(bf16[1,128,2048]{2,1,0:T(8,128)(2,1)} %param.27) | copy-start | bytes 1572868
  7.2 5.3 %copy-start.2 = (bf16[256,2048]{1,0:T(8,128)(2,1)S(1)}, bf16[256,2048]{1,0:T(8,128)(2,1)}, u32[]{:S(2)}) copy-start(bf16[256,2048]{1,0:T(8,128)(2,1)} %param.21) | copy-start | bytes 3145732
  7.2 75.2 %all-gather.4.cloned.1.call-start = ((), (), s32[]{:S(2)}) async-start(), calls=%async_computation.3 | async-start | bytes 4456448 | tf_op jit(solution)/shard_map/all_gather | solution.py:85
  13.5 68.9 %copy-start.5 = (bf16[1,2048,128]{2,1,0:T(8,128)(2,1)S(1)}, bf16[1,2048,128]{2,1,0:T(8,128)(2,1)}, u32[]{:S(2)}) copy-start(bf16[1,2048,128]{2,1,0:T(8,128)(2,1)} %param.25) | copy-start | bytes 1572868
  40.3 116.6 %reduce-scatter.2.cloned.1.call-start = ((), (), s32[]{:S(2)}) async-start(), calls=%async_computation.4 | async-start | bytes 4456448 | tf_op jit(solution)/shard_map/reduce_scatter | solution.py:90
  82.4 3.5 copy-start.6
  94.4 1.0 copy-start.3
  94.4 1.3 copy-start.9
  94.4 1.3 copy-start.13
  94.4 1.7 copy-start.14
  95.5 4.5 %copy-start.10 = (s32[256,2]{0,1:T(2,128)S(1)}, s32[256,2]{0,1:T(2,128)}, u32[]{:S(2)}) copy-start(s32[256,2]{0,1:T(2,128)} %param.23) | copy-start | bytes 6148
  95.5 72.3 %copy-start.12 = (f32[3,64]{1,0:T(4,128)S(1)}, f32[3,64]{1,0:T(4,128)}, u32[]{:S(2)}) copy-start(f32[3,64]{1,0:T(4,128)} %param.19) | copy-start | bytes 2308
  95.5 72.5 %copy-start.11 = (f32[256,2]{0,1:T(2,128)S(1)}, f32[256,2]{0,1:T(2,128)}, u32[]{:S(2)}) copy-start(f32[256,2]{0,1:T(2,128)} %param.24) | copy-start | bytes 6148
  95.6 72.5 %copy-start.7 = (bf16[64,2048]{1,0:T(8,128)(2,1)S(1)}, bf16[64,2048]{1,0:T(8,128)(2,1)}, u32[]{:S(2)}) copy-start(bf16[64,2048]{1,0:T(8,128)(2,1)} %param.20) | copy-start | bytes 786436
  95.7 72.5 %copy-start.8 = (bf16[2048,64]{0,1:T(8,128)(2,1)S(1)}, bf16[2048,64]{0,1:T(8,128)(2,1)}, u32[]{:S(2)}) copy-start(bf16[2048,64]{0,1:T(8,128)(2,1)} %param.18) | copy-start | bytes 786436
  96.5 71.6 %collective-permute-start = (bf16[2,64]{0,1:T(8,128)(2,1)S(1)}, bf16[2,64]{0,1:T(8,128)(2,1)S(1)}, u32[]{:S(2)}, u32[]{:S(2)}) collective-permute-start(bf16[2,64]{0,1:T(8,128)(2,1)S(1)} %slice.70), channel_id=1, source_target_pairs={{0,16},{16,32},{32,48},{48,64},{64,80},{80,96},{96,112},{112,128},... | collective-permute-start | bytes 776 | tf_op jit(solution)/shard_map/ppermute | solution.py:10
  158.8 19.2 %all-to-all-start.1 = ((bf16[2,32,2048]{2,0,1:T(2,128)(2,1)}), bf16[2,32,2048]{2,0,1:T(2,128)(2,1)S(1)}, u32[]{:S(2)}, u32[]{:S(2)}) async-start(bf16[2,32,2048]{2,0,1:T(2,128)(2,1)} %copy.82), calls=%async_computation.2 | async-start | bytes 524288 | tf_op jit(solution)/shard_map/all_to_all | solution.py:96
  167.5 162.6 %all-gather.6.cloned.1.call-start = ((), (), s32[]{:S(2)}) async-start(), calls=%async_computation.5 | async-start | bytes 26738688 | tf_op jit(solution)/shard_map/all_gather | solution.py:17
  392.5 2.4 copy-start.1
  392.5 1.3 copy-start.4
Sparse Core Ops, SparseCore 0:
  40.4 42.0 all-gather.3
  94.6 62.2 reduce-scatter.1
  194.8 135.2 all-gather.5
